TPU v7x, 32 devices: a whole 2x2x4 slice. The times are simulated.
32 devices in a mesh: kv: 8 (over z, y), tp: 4 (over x, core).
Axes of the slice: x: 2, y: 2, z: 4, core: 2. Of those that a mesh axis runs over, the one named last changes fastest.
Arguments:
- tokens: bfloat16 [4096, 2048], P('kv', 'tp'), may hold values from -9 to 9
- w_query: bfloat16 [2048, 1536], P(None, 'tp'), may hold values from -1 to 1
- w_key: bfloat16 [2048, 1536], P(None, 'tp'), may hold values from -1 to 1
- w_value: bfloat16 [2048, 1536], P(None, 'tp'), may hold values from -0.5 to 0.5
- w_out: bfloat16 [1536, 2048], P('tp'), may hold values from -0.15625 to 0.15625
- chosen: int32 [128, 24], P('kv'), may hold values from 0 to 127, as said below
Outputs:
- mixed: bfloat16 [4096, 2048], P(('kv', 'tp'))
Inputs may be any that keep to these rules, and one draw needn't show every extreme that they name: `chosen`: row c names blocks no later than c; its first entry is c and its second c - 1 (0 for row 0), and an entry may repeat. Taking the rows in aligned runs of 16, one run for each index of kv, the rows of one run name at most 2 distinct blocks lying in any one other index's positions; in every draw some index of kv names exactly 2 from every earlier index. Every run names some block of the index just before it and of the index half the axis before it, where those exist.
All inputs are finite; a program needn't handle non-finite values.
Results may differ from a plain program's by a relative error of at most 0.014.
Values may be sent and summed in bfloat16 or wider, within the bound.
A program may use at most 320 MiB of HBM per device.

v0:
```python
import jax
import jax.numpy as jnp
from jax import lax
from jax.sharding import PartitionSpec as P

HD = 128
BLK = 32
MOST = 2
NEG = -1e30


def attend(query_rows, key_rows, value_rows, block_ids, chosen, first_block):
    tok_rows, width = query_rows.shape
    head_count = width // HD
    key_count = key_rows.shape[0]
    slot_count = key_count // BLK
    query_blocks = tok_rows // BLK
    seen = (
        jnp.any(chosen[:, :, None] == block_ids[None, None, :], axis=1) & (block_ids >= 0)[None, :]
    )
    grid = jnp.broadcast_to(seen[:, None, :, None], (query_blocks, BLK, slot_count, BLK)).reshape(
        tok_rows, key_count
    )
    key_pos = (block_ids[:, None] * BLK + jnp.arange(BLK, dtype=jnp.int32)[None, :]).reshape(
        key_count
    )
    query_pos = first_block * BLK + jnp.arange(tok_rows, dtype=jnp.int32)
    allowed = grid & (key_pos[None, :] <= query_pos[:, None])
    query_heads = query_rows.reshape(tok_rows, head_count, HD)
    key_heads = key_rows.reshape(key_count, head_count, HD)
    value_heads = value_rows.reshape(key_count, head_count, HD)
    scores = jnp.einsum(
        "qhd,khd->hqk", query_heads, key_heads, preferred_element_type=jnp.float32
    ) * HD ** (-0.5)
    scores = jnp.where(allowed[None], scores, NEG)
    highest = jnp.max(scores, axis=-1)
    weights = jnp.where(allowed[None], jnp.exp(scores - highest[..., None]), 0.0)
    totals = jnp.sum(weights, axis=-1)
    summed = jnp.einsum("hqk,khd->hqd", weights, value_heads.astype(jnp.float32))
    return (highest, totals, summed)


def combine(left, right):
    highest = jnp.maximum(left[0], right[0])
    left_scale = jnp.exp(left[0] - highest)
    right_scale = jnp.exp(right[0] - highest)
    totals = left[1] * left_scale + right[1] * right_scale
    summed = left[2] * left_scale[..., None] + right[2] * right_scale[..., None]
    return (highest, totals, summed)


def local(tokens, w_query, w_key, w_value, w_out, chosen):
    tok_rows = tokens.shape[0]
    width = w_query.shape[1]
    empty = jnp.zeros((tok_rows, width), jnp.float32)
    totals = (empty, empty, empty)
    piece = lax.all_gather(tokens, "tp", axis=1, tiled=True)
    outputs = []
    for total, weight in zip(totals, (w_query, w_key, w_value)):
        rows = weight
        outputs.append(jnp.dot(piece, rows, preferred_element_type=jnp.float32))
    query_full, key_full, value_full = tuple(outputs)
    query_rows = query_full.astype(jnp.bfloat16)
    key_rows = key_full.astype(jnp.bfloat16)
    value_rows = value_full.astype(jnp.bfloat16)
    per_dev = tok_rows // BLK
    my_index = lax.axis_index("kv")
    first_block = my_index * per_dev
    own_ids = first_block + jnp.arange(per_dev, dtype=jnp.int32)
    own_part = attend(query_rows, key_rows, value_rows, own_ids, chosen, first_block)
    peers = lax.axis_size("kv")
    block_total = peers * per_dev
    wanted = jnp.any(
        chosen[:, :, None] == jnp.arange(block_total, dtype=jnp.int32)[None, None, :], axis=(0, 1)
    )
    peer_ids = jnp.arange(peers, dtype=jnp.int32)
    wanted = wanted.reshape(peers, per_dev) & (peer_ids != my_index)[:, None]
    ranks = jnp.cumsum(wanted.astype(jnp.int32), axis=1) - 1
    slot_hit = wanted[:, :, None] & (
        ranks[:, :, None] == jnp.arange(MOST, dtype=jnp.int32)[None, None, :]
    )
    local_ids = jnp.sum(
        slot_hit.astype(jnp.int32) * jnp.arange(per_dev, dtype=jnp.int32)[None, :, None], axis=1
    )
    present = jnp.any(slot_hit, axis=1)
    request = jnp.where(present, local_ids, -1)
    asked = lax.all_to_all(request, "kv", split_axis=0, concat_axis=0, tiled=True)
    picked = jnp.clip(asked, 0).reshape(-1)
    send_keys = key_rows.reshape(per_dev, BLK, width)[picked]
    send_values = value_rows.reshape(per_dev, BLK, width)[picked]
    got_keys, got_values = (
        lax.all_to_all(send_keys, "kv", split_axis=0, concat_axis=0, tiled=True),
        lax.all_to_all(send_values, "kv", split_axis=0, concat_axis=0, tiled=True),
    )
    got_ids = jnp.where(present, peer_ids[:, None] * per_dev + local_ids, -1).reshape(-1)
    far_part = attend(
        query_rows,
        got_keys.reshape(-1, width),
        got_values.reshape(-1, width),
        got_ids,
        chosen,
        first_block,
    )
    merged = combine(own_part, far_part)
    normed = merged[2] / merged[1][..., None]
    attended = jnp.transpose(normed, (1, 0, 2)).reshape(tok_rows, width).astype(jnp.bfloat16)
    rows = attended
    return lax.psum_scatter(
        jnp.dot(rows, w_out, preferred_element_type=jnp.float32).astype(jnp.bfloat16),
        "tp",
        scatter_dimension=0,
        tiled=True,
    )


def solution(mesh):
    return jax.shard_map(
        local,
        mesh=mesh,
        in_specs=(
            P("kv", "tp"),
            P(None, "tp"),
            P(None, "tp"),
            P(None, "tp"),
            P("tp", None),
            P("kv", None),
        ),
        out_specs=P(("kv", "tp"), None),
        check_vma=False,
    )
```

profile of v0, /device:TPU:0, one launch (start us, length us, event | category | flops | bytes accessed | tf_op | source)
XLA Modules:
  0.0 118.5 jit_solution(13071488536581529827)
XLA Ops:
  6.5 0.0 copy-start
  6.5 0.0 all-gather.2.cloned.1.call-start
  6.5 0.7 all-gather.2.cloned.1.call-update
  7.3 0.8 fusion.26
  8.1 0.1 reshape.337
  8.2 0.1 fusion.40
  8.3 0.2 reduce_window_sum.11
  8.4 0.2 fusion.31
  8.6 0.2 select_reduce_fusion
  8.8 0.7 copy.46
  9.4 7.3 %all-to-all-start = ((s32[8,1,2]{2,1,0:T(1,128)}), s32[8,1,2]{2,1,0:T(1,128)S(1)}, u32[]{:S(2)}, u32[]{:S(2)}) async-start(s32[8,1,2]{2,1,0:T(1,128)} %copy.46), calls=%async_computation | async-start | bytes 8192 | tf_op jit(solution)/shard_map/all_to_all | solution.py:87
  16.7 0.1 copy.44
  16.8 0.1 select_n.53
  16.9 1.4 %compare_reduce_fusion = (pred[16,16]{1,0:T(8,128)(4,1)S(1)}, pred[16,16]{1,0:T(8,128)(4,1)S(1)}) fusion(s32[16,24]{1,0:T(8,128)} %param.11, s32[16]{0:T(128)S(1)} %select_n.53, s32[16]{0:T(128)S(1)} %get-tuple-element.20), kind=kLoop, calls=%fused_computation.40 | loop fusion | flops 24064 | bytes 2176 | tf_op jit(solution)/shard_map/reduce_or | solution.py:19
  18.3 0.1 copy.45
  18.4 0.3 broadcast_in_dim.42
  18.8 2.1 %reshape.338 = pred[512,512]{0,1:T(8,128)(4,1)S(1)} reshape(pred[16,32,16,32]{1,0,3,2:T(8,128)(4,1)S(1)} %broadcast_in_dim.42) | data formatting | bytes 524288 | tf_op jit(solution)/shard_map/reshape | solution.py:21
  20.9 0.1 iota_add_fusion
  21.0 0.1 add.128
  21.1 0.1 copy.38
  21.2 0.3 broadcast_in_dim.37
  21.5 2.1 %reshape.333 = pred[512,512]{0,1:T(8,128)(4,1)S(1)} reshape(pred[16,32,16,32]{1,0,3,2:T(8,128)(4,1)S(1)} %broadcast_in_dim.37) | data formatting | bytes 524288 | tf_op jit(solution)/shard_map/reshape | solution.py:21
  23.6 0.1 iota_add_fusion.1
  23.7 0.1 add.120
  23.8 0.5 compare_and_fusion
  24.3 0.0 all-to-all-done
  24.3 0.1 reshape.343
  24.4 9.8 %all-gather.2.cloned.1.call-done = bf16[512,2048]{1,0:T(8,128)(2,1)} async-done(((bf16[512,512]{1,0:T(8,128)(2,1)}), bf16[512,2048]{1,0:T(8,128)(2,1)}) %all-gather.2.cloned.1.call-update) | async-done | bytes 2097168 | tf_op jit(solution)/shard_map/all_gather | solution.py:57
  34.2 3.3 %convolution_convert_fusion.1 = bf16[512,384]{1,0:T(8,128)(2,1)S(1)} fusion(bf16[512,2048]{1,0:T(8,128)(2,1)} %all-gather.2.cloned.1.call-done, bf16[2048,384]{1,0:T(8,128)(2,1)} %param.9), kind=kOutput, calls=%fused_computation.28 | convolution fusion | flops 805502976 | bytes 4063232 | tf_op jit(solution)/shard_map/dot_general | solution.py:61
  37.5 0.9 copy.42
  38.4 3.3 %convolution_convert_fusion.2 = bf16[512,384]{1,0:T(8,128)(2,1)S(1)} fusion(bf16[512,2048]{1,0:T(8,128)(2,1)} %all-gather.2.cloned.1.call-done, bf16[2048,384]{1,0:T(8,128)(2,1)} %param.8), kind=kOutput, calls=%fused_computation.29 | convolution fusion | flops 805502976 | bytes 4063232 | tf_op jit(solution)/shard_map/dot_general | solution.py:61
  41.7 0.2 copy.39
  41.9 1.3 %gather_fusion = bf16[16,32,384]{2,1,0:T(8,128)(2,1)} fusion(bf16[16,32,384]{2,1,0:T(8,128)(2,1)S(1)} %bitcast.62, s32[1024]{0:T(1024)S(1)} %pad_clamp_fusion), kind=kCustom, calls=%fused_computation | custom fusion | bytes 786496 | tf_op jit(solution)/shard_map/gather | solution.py:89
  43.3 5.5 %all-to-all-start.1 = ((bf16[16,32,384]{2,1,0:T(8,128)(2,1)}), bf16[16,32,384]{2,1,0:T(8,128)(2,1)S(1)}, u32[]{:S(2)}, u32[]{:S(2)}) async-start(bf16[16,32,384]{2,1,0:T(8,128)(2,1)} %gather_fusion), calls=%async_computation.1 | async-start | bytes 786432 | tf_op jit(solution)/shard_map/all_to_all | solution.py:92
  48.8 1.4 %gather_fusion.1 = bf16[16,32,384]{2,1,0:T(8,128)(2,1)} fusion(bf16[16,32,384]{2,1,0:T(8,128)(2,1)S(1)} %bitcast.61, s32[1024]{0:T(1024)S(1)} %pad_clamp_fusion), kind=kCustom, calls=%fused_computation.1 | custom fusion | bytes 786496 | tf_op jit(solution)/shard_map/gather | solution.py:90
  50.2 3.1 %convolution_convert_fusion.3 = bf16[512,384]{0,1:T(8,128)(2,1)S(1)} fusion(bf16[512,2048]{1,0:T(8,128)(2,1)} %all-gather.2.cloned.1.call-done, bf16[2048,384]{1,0:T(8,128)(2,1)} %param.7), kind=kOutput, calls=%fused_computation.30 | convolution fusion | flops 805502976 | bytes 4063232 | tf_op jit(solution)/shard_map/dot_general | solution.py:61
  53.2 0.0 copy-start.4
  53.2 0.8 fusion
  54.0 0.0 copy-start.1
  54.1 1.7 %copy-done.1 = f32[3,512,512]{1,2,0:T(8,128)} copy-done((f32[3,512,512]{1,2,0:T(8,128)}, f32[3,512,512]{1,2,0:T(8,128)S(1)}, u32[]{:S(2)}) %copy-start.1) | copy-done | bytes 3145752
  55.7 0.8 fusion.2
  56.5 4.3 %all-to-all-done.1 = bf16[16,32,384]{2,1,0:T(8,128)(2,1)S(1)} async-done(((bf16[16,32,384]{2,1,0:T(8,128)(2,1)}), bf16[16,32,384]{2,1,0:T(8,128)(2,1)S(1)}, u32[]{:S(2)}, u32[]{:S(2)}) %all-to-all-start.1) | async-done | bytes 393248 | tf_op jit(solution)/shard_map/all_to_all | solution.py:92
  60.9 3.6 %all-to-all-start.2 = ((bf16[16,32,384]{2,1,0:T(8,128)(2,1)}), bf16[16,32,384]{2,1,0:T(8,128)(2,1)S(1)}, u32[]{:S(2)}, u32[]{:S(2)}) async-start(bf16[16,32,384]{2,1,0:T(8,128)(2,1)} %gather_fusion.1), calls=%async_computation.2 | async-start | bytes 786432 | tf_op jit(solution)/shard_map/all_to_all | solution.py:93
  64.5 0.0 copy-done.4
  64.5 0.2 reduce-scatter.2.cloned.1.call-start
  64.7 0.1 reshape_reshape.6
  64.8 0.0 copy-start.2
  64.9 0.0 copy-start.5
  64.9 1.9 %fusion.1 = (f32[3,512]{1,0:T(4,128)S(1)}, f32[3,512,512]{1,2,0:T(8,128)S(1)}) fusion(pred[512,512]{0,1:T(8,128)(4,1)S(1)} %get-tuple-element.12, bf16[512,3,128]{0,2,1:T(8,128)(2,1)} %bitcast.64, bf16[512,3,128]{2,1,0:T(4,128)(2,1)S(1)} %reshape_reshape.6), kind=kOutput, calls=%fused_computation.8 | convolution fusion | flops 203684352 | bytes 4200448 | tf_op jit(solution)/shard_map/qhd,khd->hqk/dot_general | solution.py:32
  66.8 0.0 copy-start.3
  66.8 1.7 %copy-done.3 = f32[3,512,512]{1,2,0:T(8,128)} copy-done((f32[3,512,512]{1,2,0:T(8,128)}, f32[3,512,512]{1,2,0:T(8,128)S(1)}, u32[]{:S(2)}) %copy-start.3) | copy-done | bytes 3145752
  68.5 0.8 fusion.4
  69.3 0.0 copy-done.2
  69.3 0.0 copy-done.5
  69.3 1.9 %fusion.18 = f32[512,3,128]{0,2,1:T(8,128)} fusion(bf16[512,3,128]{0,2,1:T(8,128)(2,1)S(1)} %bitcast.65, f32[3,512,512]{1,2,0:T(8,128)S(1)} %copy-done.2, f32[3,512]{1,0:T(4,128)S(1)} %get-tuple-element.16, pred[512,512]{0,1:T(8,128)(4,1)S(1)} %get-tuple-element.13, f32[512,3]{0,1:T(4,128)S(1)} %get-tuple-element.9), kind=kOutput, calls=%fused_computation.25 | convolution fusion | flops 204668928 | bytes 4599808 | tf_op jit(solution)/shard_map/hqk,khd->hqd/dot_general | solution.py:39
  71.2 5.2 %all-to-all-done.2 = bf16[16,32,384]{2,1,0:T(8,128)(2,1)S(1)} async-done(((bf16[16,32,384]{2,1,0:T(8,128)(2,1)}), bf16[16,32,384]{2,1,0:T(8,128)(2,1)S(1)}, u32[]{:S(2)}, u32[]{:S(2)}) %all-to-all-start.2) | async-done | bytes 393248 | tf_op jit(solution)/shard_map/all_to_all | solution.py:93
  76.4 0.1 reshape_reshape.7
  76.5 3.1 %fusion.22 = bf16[512,3,128]{0,2,1:T(8,128)(2,1)S(1)} fusion(f32[512,3,128]{0,2,1:T(8,128)} %fusion.18, f32[3,512,512]{1,2,0:T(8,128)} %copy-done.3, f32[3,512]{1,0:T(4,128)S(1)} %get-tuple-element.18, pred[512,512]{0,1:T(8,128)(4,1)S(1)} %get-tuple-element.12, bf16[512,3,128]{2,1,0:T(4,128)(2,1)S(1)} %reshape_reshape.7, ...), kind=kOutput, calls=%fused_computation.34 | convolution fusion | flops 205258752 | bytes 4999168 | tf_op jit(solution)/shard_map/hqk,khd->hqd/dot_general | solution.py:39
  79.6 0.0 copy-done
  79.6 2.7 %convolution_convert_fusion = bf16[512,2048]{1,0:T(8,128)(2,1)} fusion(bf16[512,384]{0,1:T(8,128)(2,1)S(1)} %bitcast.66, bf16[384,2048]{1,0:T(8,128)(2,1)S(1)} %copy-done), kind=kOutput, calls=%fused_computation.6 | convolution fusion | flops 806354944 | bytes 4063232 | tf_op jit(solution)/shard_map/dot_general | solution.py:109
  82.2 0.0 reduce-scatter.2.cloned.1.call-update
  82.3 29.4 %reduce-scatter.2.cloned.1.call-done = bf16[128,2048]{1,0:T(8,128)(2,1)} async-done(((bf16[512,2048]{1,0:T(8,128)(2,1)}), bf16[128,2048]{1,0:T(8,128)(2,1)}) %reduce-scatter.2.cloned.1.call-update) | async-done | bytes 524304 | tf_op jit(solution)/shard_map/reduce_scatter | solution.py:108
  (14 shorter events, 0.1 us)
Async XLA Ops:
  6.5 73.0 %copy-start = (bf16[384,2048]{1,0:T(8,128)(2,1)S(1)}, bf16[384,2048]{1,0:T(8,128)(2,1)}, u32[]{:S(2)}) copy-start(bf16[384,2048]{1,0:T(8,128)(2,1)} %param.10) | copy-start | bytes 4718596
  6.5 27.7 %all-gather.2.cloned.1.call-start = ((), (), s32[]{:S(2)}) async-start(), calls=%async_computation.4 | async-start | bytes 2621440 | tf_op jit(solution)/shard_map/all_gather | solution.py:57
  9.4 14.8 %all-to-all-start = ((s32[8,1,2]{2,1,0:T(1,128)}), s32[8,1,2]{2,1,0:T(1,128)S(1)}, u32[]{:S(2)}, u32[]{:S(2)}) async-start(s32[8,1,2]{2,1,0:T(1,128)} %copy.46), calls=%async_computation | async-start | bytes 8192 | tf_op jit(solution)/shard_map/all_to_all | solution.py:87
  43.3 17.6 %all-to-all-start.1 = ((bf16[16,32,384]{2,1,0:T(8,128)(2,1)}), bf16[16,32,384]{2,1,0:T(8,128)(2,1)S(1)}, u32[]{:S(2)}, u32[]{:S(2)}) async-start(bf16[16,32,384]{2,1,0:T(8,128)(2,1)} %gather_fusion), calls=%async_computation.1 | async-start | bytes 786432 | tf_op jit(solution)/shard_map/all_to_all | solution.py:92
  53.2 11.3 %copy-start.4 = (bf16[512,384]{0,1:T(8,128)(2,1)}, bf16[512,384]{0,1:T(8,128)(2,1)S(1)}, u32[]{:S(2)}) copy-start(bf16[512,384]{0,1:T(8,128)(2,1)S(1)} %convolution_convert_fusion.3) | copy-start | bytes 1179652
  54.0 1.7 %copy-start.1 = (f32[3,512,512]{1,2,0:T(8,128)}, f32[3,512,512]{1,2,0:T(8,128)S(1)}, u32[]{:S(2)}) copy-start(f32[3,512,512]{1,2,0:T(8,128)S(1)} %get-tuple-element.17) | copy-start | bytes 9437188
  60.9 15.5 %all-to-all-start.2 = ((bf16[16,32,384]{2,1,0:T(8,128)(2,1)}), bf16[16,32,384]{2,1,0:T(8,128)(2,1)S(1)}, u32[]{:S(2)}, u32[]{:S(2)}) async-start(bf16[16,32,384]{2,1,0:T(8,128)(2,1)} %gather_fusion.1), calls=%async_computation.2 | async-start | bytes 786432 | tf_op jit(solution)/shard_map/all_to_all | solution.py:93
  64.5 47.2 %reduce-scatter.2.cloned.1.call-start = ((), (), s32[]{:S(2)}) async-start(), calls=%async_computation.5 | async-start | bytes 2621440 | tf_op jit(solution)/shard_map/reduce_scatter | solution.py:108
  64.8 4.5 %copy-start.2 = (f32[3,512,512]{1,2,0:T(8,128)S(1)}, f32[3,512,512]{1,2,0:T(8,128)}, u32[]{:S(2)}) copy-start(f32[3,512,512]{1,2,0:T(8,128)} %copy-done.1) | copy-start | bytes 9437188
  64.9 4.5 %copy-start.5 = (bf16[512,384]{0,1:T(8,128)(2,1)S(1)}, bf16[512,384]{0,1:T(8,128)(2,1)}, u32[]{:S(2)}) copy-start(bf16[512,384]{0,1:T(8,128)(2,1)} %copy.42) | copy-start | bytes 1179652
  66.8 1.7 %copy-start.3 = (f32[3,512,512]{1,2,0:T(8,128)}, f32[3,512,512]{1,2,0:T(8,128)S(1)}, u32[]{:S(2)}) copy-start(f32[3,512,512]{1,2,0:T(8,128)S(1)} %get-tuple-element.19) | copy-start | bytes 9437188
Sparse Core Ops, SparseCore 0:
  8.9 25.2 all-gather.1
  82.4 29.2 reduce-scatter.1
where the time goes:
time: 119 us
  waiting for transfers between devices  49.5 us (42%)
  matrix products  19.9 us (17%)
  starting transfers between devices  16.7 us (14%)
  local copies, waits for them, and re-layouts  13.7 us (12%)
  between operations  13.6 us (11%)
  other arithmetic  5.12 us (4%)
    reduce_scatter x1, waiting for transfers between devices, local(): lax.psum_scatter(jnp.dot(rows, w_out, preferred_element_type=jnp.float32)...  29.4 us
    all_gather x1, waiting for transfers between devices, local(): piece = lax.all_gather(tokens, 'tp', axis=1, tiled=True)  9.83 us
    dot_general x3, matrix products, local(): outputs.append(jnp.dot(piece, rows, preferred_element_type=jnp.float32))  9.62 us
    all_to_all x1, starting transfers between devices, local(): lax.all_to_all(request, 'kv', split_axis=0, concat_axis=0, tiled=True)  7.31 us
    all_to_all x1, starting transfers between devices, local(): lax.all_to_all(send_keys, 'kv', split_axis=0, concat_axis=0, tiled=True)  5.51 us
    all_to_all x1, waiting for transfers between devices, local(): lax.all_to_all(send_values, 'kv', split_axis=0, concat_axis=0, tiled=True)  5.16 us
    dot_general x2, matrix products, attend(): jnp.einsum('hqk,khd->hqd', weights, value_heads.astype(jnp.float32))  4.96 us
    all_to_all x1, waiting for transfers between devices, local(): lax.all_to_all(send_keys, 'kv', split_axis=0, concat_axis=0, tiled=True)  4.32 us
  transfers between devices with their start and end apart: 5, of which 4 were waited for; matrix products, arithmetic and copies ran while one was open for 17% of the time, Pallas kernels for 0%

commit v1 on v0

--- a/solution.py
+++ b/solution.py
@@ -54,7 +54,7 @@
     width = w_query.shape[1]
     empty = jnp.zeros((tok_rows, width), jnp.float32)
     totals = (empty, empty, empty)
-    piece = lax.all_gather(tokens, "tp", axis=1, tiled=True)
+    piece = jnp.concatenate(lax.all_gather(tokens, axis_name="tp"), 1)
     outputs = []
     for total, weight in zip(totals, (w_query, w_key, w_value)):
         rows = weight

time: 119 us -> 125 us (1.050)
  local copies, waits for them, and re-layouts: 13.7 us -> 17.8 us
  waiting for transfers between devices: 49.5 us -> 51.5 us
    reshape x0 -> x1, local copies, waits for them, and re-layouts: none -> 4.14 us  [local(): piece = jnp.concatenate(lax.all_gather(tokens, axis_name='tp'), 1)]
    all_to_all x1, waiting for transfers between devices: 4.32 us -> 6.4 us  [local(): lax.all_to_all(send_keys, 'kv', split_axis=0, concat_axis=0, tiled=True)]
    unnamed x12 -> x14, local copies, waits for them, and re-layouts: 3.37 us -> 3.38 us
  transfers between devices with their start and end apart: 5 -> 5, of which waited for: 4 -> 4; matrix products, arithmetic and copies ran while one was open for 17% -> 15% of each run, Pallas kernels for 0% -> 0%
where the time goes in v1:
time: 125 us
  waiting for transfers between devices  51.5 us (41%)
  matrix products  19.9 us (16%)
  local copies, waits for them, and re-layouts  17.8 us (14%)
  starting transfers between devices  16.7 us (13%)
  between operations  13.6 us (11%)
  other arithmetic  5.12 us (4%)
    reduce_scatter x1, waiting for transfers between devices, local(): lax.psum_scatter(jnp.dot(rows, w_out, preferred_element_type=jnp.float32)...  29.4 us
    all_gather x1, waiting for transfers between devices, local(): piece = jnp.concatenate(lax.all_gather(tokens, axis_name='tp'), 1)  9.82 us
    dot_general x3, matrix products, local(): outputs.append(jnp.dot(piece, rows, preferred_element_type=jnp.float32))  8.55 us
    all_to_all x1, starting transfers between devices, local(): lax.all_to_all(request, 'kv', split_axis=0, concat_axis=0, tiled=True)  7.31 us
    all_to_all x1, waiting for transfers between devices, local(): lax.all_to_all(send_keys, 'kv', split_axis=0, concat_axis=0, tiled=True)  6.4 us
    all_to_all x1, starting transfers between devices, local(): lax.all_to_all(send_keys, 'kv', split_axis=0, concat_axis=0, tiled=True)  5.51 us
    all_to_all x1, waiting for transfers between devices, local(): lax.all_to_all(send_values, 'kv', split_axis=0, concat_axis=0, tiled=True)  5.17 us
    dot_general x2, matrix products, attend(): jnp.einsum('hqk,khd->hqd', weights, value_heads.astype(jnp.float32))  4.95 us
  transfers between devices with their start and end apart: 5, of which 4 were waited for; matrix products, arithmetic and copies ran while one was open for 15% of the time, Pallas kernels for 0%

profile of v1, /device:TPU:0, one launch (start us, length us, event | category | flops | bytes accessed | tf_op | source)
XLA Modules:
  0.0 124.6 jit_solution(4643638261088283786)
XLA Ops:
  6.5 0.0 copy-start
  6.5 0.0 all-gather.3.cloned.1.call-start
  6.5 0.7 all-gather.3.cloned.1.call-update
  7.3 0.8 fusion.26
  8.1 0.1 reshape.345
  8.2 0.1 fusion.40
  8.3 0.2 reduce_window_sum.11
  8.4 0.2 fusion.31
  8.6 0.2 select_reduce_fusion
  8.8 0.7 copy.60
  9.4 7.3 %all-to-all-start = ((s32[8,1,2]{2,1,0:T(1,128)}), s32[8,1,2]{2,1,0:T(1,128)S(1)}, u32[]{:S(2)}, u32[]{:S(2)}) async-start(s32[8,1,2]{2,1,0:T(1,128)} %copy.60), calls=%async_computation | async-start | bytes 8192 | tf_op jit(solution)/shard_map/all_to_all | solution.py:87
  16.7 0.1 copy.58
  16.8 0.1 select_n.53
  16.9 1.4 %compare_reduce_fusion = (pred[16,16]{1,0:T(8,128)(4,1)S(1)}, pred[16,16]{1,0:T(8,128)(4,1)S(1)}) fusion(s32[16,24]{1,0:T(8,128)} %param.11, s32[16]{0:T(128)S(1)} %select_n.53, s32[16]{0:T(128)S(1)} %get-tuple-element.20), kind=kLoop, calls=%fused_computation.40 | loop fusion | flops 24064 | bytes 2176 | tf_op jit(solution)/shard_map/reduce_or | solution.py:19
  18.3 0.1 copy.59
  18.4 0.3 broadcast_in_dim.42
  18.8 2.1 %reshape.346 = pred[512,512]{0,1:T(8,128)(4,1)S(1)} reshape(pred[16,32,16,32]{1,0,3,2:T(8,128)(4,1)S(1)} %broadcast_in_dim.42) | data formatting | bytes 524288 | tf_op jit(solution)/shard_map/reshape | solution.py:21
  20.9 0.1 iota_add_fusion
  21.0 0.1 add.128
  21.1 0.1 copy.51
  21.2 0.3 broadcast_in_dim.37
  21.5 2.1 %reshape.339 = pred[512,512]{0,1:T(8,128)(4,1)S(1)} reshape(pred[16,32,16,32]{1,0,3,2:T(8,128)(4,1)S(1)} %broadcast_in_dim.37) | data formatting | bytes 524288 | tf_op jit(solution)/shard_map/reshape | solution.py:21
  23.6 0.1 iota_add_fusion.1
  23.7 0.1 add.120
  23.8 0.5 compare_and_fusion
  24.3 0.0 all-to-all-done
  24.3 0.1 reshape.351
  24.4 9.8 %all-gather.3.cloned.1.call-done = bf16[2048,512]{1,0:T(8,128)(2,1)} async-done(((bf16[512,512]{1,0:T(8,128)(2,1)}), bf16[2048,512]{1,0:T(8,128)(2,1)}) %all-gather.3.cloned.1.call-update) | async-done | bytes 2097168 | tf_op jit(solution)/shard_map/all_gather | solution.py:57
  34.2 4.1 %copy.52 = bf16[512,4,512]{0,2,1:T(8,128)(2,1)} copy(bf16[512,4,512]{2,0,1:T(8,128)(2,1)} %bitcast.69) | data formatting | bytes 4194304 | tf_op jit(solution)/shard_map/reshape | solution.py:57
  38.4 3.3 %convolution_convert_fusion.1 = bf16[512,384]{1,0:T(8,128)(2,1)S(1)} fusion(bf16[512,2048]{0,1:T(8,128)(2,1)} %bitcast.64, bf16[2048,384]{1,0:T(8,128)(2,1)} %param.9), kind=kOutput, calls=%fused_computation.28 | convolution fusion | flops 805502976 | bytes 4063232 | tf_op jit(solution)/shard_map/dot_general | solution.py:61
  41.7 0.9 copy.56
  42.6 0.0 copy-start.1
  42.6 4.0 %convolution_convert_fusion.3 = bf16[512,384]{0,1:T(8,128)(2,1)} fusion(bf16[512,2048]{0,1:T(8,128)(2,1)} %bitcast.65, bf16[2048,384]{1,0:T(8,128)(2,1)} %param.7), kind=kOutput, calls=%fused_computation.30 | convolution fusion | flops 805502976 | bytes 4063232 | tf_op jit(solution)/shard_map/dot_general | solution.py:61
  46.6 0.0 copy-done.1
  46.6 0.0 copy-done.5
  46.6 1.3 %convolution_convert_fusion.2 = bf16[512,384]{1,0:T(8,128)(2,1)S(1)} fusion(bf16[512,2048]{0,1:T(8,128)(2,1)S(1)} %bitcast.66, bf16[2048,384]{1,0:T(8,128)(2,1)S(1)} %copy-done.5), kind=kOutput, calls=%fused_computation.29 | convolution fusion | flops 805502976 | bytes 4063232 | tf_op jit(solution)/shard_map/dot_general | solution.py:61
  47.9 0.2 copy.53
  48.1 1.3 %gather_fusion = bf16[16,32,384]{2,1,0:T(8,128)(2,1)} fusion(bf16[16,32,384]{2,1,0:T(8,128)(2,1)S(1)} %bitcast.68, s32[1024]{0:T(1024)S(1)} %pad_clamp_fusion), kind=kCustom, calls=%fused_computation | custom fusion | bytes 786496 | tf_op jit(solution)/shard_map/gather | solution.py:89
  49.4 5.5 %all-to-all-start.1 = ((bf16[16,32,384]{2,1,0:T(8,128)(2,1)}), bf16[16,32,384]{2,1,0:T(8,128)(2,1)S(1)}, u32[]{:S(2)}, u32[]{:S(2)}) async-start(bf16[16,32,384]{2,1,0:T(8,128)(2,1)} %gather_fusion), calls=%async_computation.1 | async-start | bytes 786432 | tf_op jit(solution)/shard_map/all_to_all | solution.py:92
  54.9 1.4 %gather_fusion.1 = bf16[16,32,384]{2,1,0:T(8,128)(2,1)} fusion(bf16[16,32,384]{2,1,0:T(8,128)(2,1)S(1)} %bitcast.67, s32[1024]{0:T(1024)S(1)} %pad_clamp_fusion), kind=kCustom, calls=%fused_computation.1 | custom fusion | bytes 786496 | tf_op jit(solution)/shard_map/gather | solution.py:90
  56.3 1.8 %fusion = (f32[3,512]{1,0:T(4,128)S(1)}, f32[3,512,512]{1,2,0:T(8,128)S(1)}) fusion(pred[512,512]{0,1:T(8,128)(4,1)S(1)} %get-tuple-element.13, bf16[512,3,128]{0,2,1:T(8,128)(2,1)} %bitcast.71, bf16[512,3,128]{0,2,1:T(8,128)(2,1)S(1)} %bitcast.70), kind=kOutput, calls=%fused_computation.7 | convolution fusion | flops 203684352 | bytes 4200448 | tf_op jit(solution)/shard_map/qhd,khd->hqk/dot_general | solution.py:32
  58.1 0.0 copy-start.2
  58.1 1.7 %copy-done.2 = f32[3,512,512]{1,2,0:T(8,128)} copy-done((f32[3,512,512]{1,2,0:T(8,128)}, f32[3,512,512]{1,2,0:T(8,128)S(1)}, u32[]{:S(2)}) %copy-start.2) | copy-done | bytes 3145752
  59.8 0.8 fusion.2
  60.6 6.4 %all-to-all-done.1 = bf16[16,32,384]{2,1,0:T(8,128)(2,1)S(1)} async-done(((bf16[16,32,384]{2,1,0:T(8,128)(2,1)}), bf16[16,32,384]{2,1,0:T(8,128)(2,1)S(1)}, u32[]{:S(2)}, u32[]{:S(2)}) %all-to-all-start.1) | async-done | bytes 393248 | tf_op jit(solution)/shard_map/all_to_all | solution.py:92
  67.0 3.6 %all-to-all-start.2 = ((bf16[16,32,384]{2,1,0:T(8,128)(2,1)}), bf16[16,32,384]{2,1,0:T(8,128)(2,1)S(1)}, u32[]{:S(2)}, u32[]{:S(2)}) async-start(bf16[16,32,384]{2,1,0:T(8,128)(2,1)} %gather_fusion.1), calls=%async_computation.2 | async-start | bytes 786432 | tf_op jit(solution)/shard_map/all_to_all | solution.py:93
  70.6 0.2 reduce-scatter.2.cloned.1.call-start
  70.9 0.1 reshape_reshape.6
  71.0 0.0 copy-start.3
  71.0 0.0 copy-start.6
  71.0 1.9 %fusion.1 = (f32[3,512]{1,0:T(4,128)S(1)}, f32[3,512,512]{1,2,0:T(8,128)S(1)}) fusion(pred[512,512]{0,1:T(8,128)(4,1)S(1)} %get-tuple-element.12, bf16[512,3,128]{0,2,1:T(8,128)(2,1)} %bitcast.72, bf16[512,3,128]{2,1,0:T(4,128)(2,1)S(1)} %reshape_reshape.6), kind=kOutput, calls=%fused_computation.8 | convolution fusion | flops 203684352 | bytes 4200448 | tf_op jit(solution)/shard_map/qhd,khd->hqk/dot_general | solution.py:32
  72.9 0.0 copy-start.4
  72.9 1.7 %copy-done.4 = f32[3,512,512]{1,2,0:T(8,128)} copy-done((f32[3,512,512]{1,2,0:T(8,128)}, f32[3,512,512]{1,2,0:T(8,128)S(1)}, u32[]{:S(2)}) %copy-start.4) | copy-done | bytes 3145752
  74.6 0.8 fusion.4
  75.4 0.0 copy-done.3
  75.4 0.0 copy-done.6
  75.4 1.9 %fusion.18 = f32[512,3,128]{0,2,1:T(8,128)} fusion(bf16[512,3,128]{0,2,1:T(8,128)(2,1)S(1)} %bitcast.73, f32[3,512,512]{1,2,0:T(8,128)S(1)} %copy-done.3, f32[3,512]{1,0:T(4,128)S(1)} %get-tuple-element.16, pred[512,512]{0,1:T(8,128)(4,1)S(1)} %get-tuple-element.13, f32[512,3]{0,1:T(4,128)S(1)} %get-tuple-element.9), kind=kOutput, calls=%fused_computation.25 | convolution fusion | flops 204668928 | bytes 4599808 | tf_op jit(solution)/shard_map/hqk,khd->hqd/dot_general | solution.py:39
  77.3 5.2 %all-to-all-done.2 = bf16[16,32,384]{2,1,0:T(8,128)(2,1)S(1)} async-done(((bf16[16,32,384]{2,1,0:T(8,128)(2,1)}), bf16[16,32,384]{2,1,0:T(8,128)(2,1)S(1)}, u32[]{:S(2)}, u32[]{:S(2)}) %all-to-all-start.2) | async-done | bytes 393248 | tf_op jit(solution)/shard_map/all_to_all | solution.py:93
  82.5 0.1 reshape_reshape.7
  82.6 3.1 %fusion.22 = bf16[512,3,128]{0,2,1:T(8,128)(2,1)S(1)} fusion(f32[512,3,128]{0,2,1:T(8,128)} %fusion.18, f32[3,512,512]{1,2,0:T(8,128)} %copy-done.4, f32[3,512]{1,0:T(4,128)S(1)} %get-tuple-element.18, pred[512,512]{0,1:T(8,128)(4,1)S(1)} %get-tuple-element.12, bf16[512,3,128]{2,1,0:T(4,128)(2,1)S(1)} %reshape_reshape.7, ...), kind=kOutput, calls=%fused_computation.34 | convolution fusion | flops 205258752 | bytes 4999168 | tf_op jit(solution)/shard_map/hqk,khd->hqd/dot_general | solution.py:39
  85.7 0.0 copy-done
  85.7 2.7 %convolution_convert_fusion = bf16[512,2048]{1,0:T(8,128)(2,1)} fusion(bf16[512,384]{0,1:T(8,128)(2,1)S(1)} %bitcast.74, bf16[384,2048]{1,0:T(8,128)(2,1)S(1)} %copy-done), kind=kOutput, calls=%fused_computation.6 | convolution fusion | flops 806354944 | bytes 4063232 | tf_op jit(solution)/shard_map/dot_general | solution.py:109
  88.4 0.0 reduce-scatter.2.cloned.1.call-update
  88.4 29.4 %reduce-scatter.2.cloned.1.call-done = bf16[128,2048]{1,0:T(8,128)(2,1)} async-done(((bf16[512,2048]{1,0:T(8,128)(2,1)}), bf16[128,2048]{1,0:T(8,128)(2,1)}) %reduce-scatter.2.cloned.1.call-update) | async-done | bytes 524304 | tf_op jit(solution)/shard_map/reduce_scatter | solution.py:108
  (15 shorter events, 0.1 us)
Async XLA Ops:
  6.5 79.2 %copy-start = (bf16[384,2048]{1,0:T(8,128)(2,1)S(1)}, bf16[384,2048]{1,0:T(8,128)(2,1)}, u32[]{:S(2)}) copy-start(bf16[384,2048]{1,0:T(8,128)(2,1)} %param.10) | copy-start | bytes 4718596
  6.5 27.7 %all-gather.3.cloned.1.call-start = ((), (), s32[]{:S(2)}) async-start(), calls=%async_computation.5 | async-start | bytes 2621440 | tf_op jit(solution)/shard_map/all_gather | solution.py:57
  9.4 14.8 %all-to-all-start = ((s32[8,1,2]{2,1,0:T(1,128)}), s32[8,1,2]{2,1,0:T(1,128)S(1)}, u32[]{:S(2)}, u32[]{:S(2)}) async-start(s32[8,1,2]{2,1,0:T(1,128)} %copy.60), calls=%async_computation | async-start | bytes 8192 | tf_op jit(solution)/shard_map/all_to_all | solution.py:87
  42.6 4.0 %copy-start.1 = (bf16[512,4,512]{0,2,1:T(8,128)(2,1)S(1)}, bf16[512,4,512]{0,2,1:T(8,128)(2,1)}, u32[]{:S(2)}) copy-start(bf16[512,4,512]{0,2,1:T(8,128)(2,1)} %copy.52) | copy-start | bytes 6291460
  42.6 4.0 %copy-start.5 = (bf16[2048,384]{1,0:T(8,128)(2,1)S(1)}, bf16[2048,384]{1,0:T(8,128)(2,1)}, u32[]{:S(2)}) copy-start(bf16[2048,384]{1,0:T(8,128)(2,1)} %param.8) | copy-start | bytes 4718596
  49.4 17.6 %all-to-all-start.1 = ((bf16[16,32,384]{2,1,0:T(8,128)(2,1)}), bf16[16,32,384]{2,1,0:T(8,128)(2,1)S(1)}, u32[]{:S(2)}, u32[]{:S(2)}) async-start(bf16[16,32,384]{2,1,0:T(8,128)(2,1)} %gather_fusion), calls=%async_computation.1 | async-start | bytes 786432 | tf_op jit(solution)/shard_map/all_to_all | solution.py:92
  58.1 1.7 %copy-start.2 = (f32[3,512,512]{1,2,0:T(8,128)}, f32[3,512,512]{1,2,0:T(8,128)S(1)}, u32[]{:S(2)}) copy-start(f32[3,512,512]{1,2,0:T(8,128)S(1)} %get-tuple-element.17) | copy-start | bytes 9437188
  67.0 15.5 %all-to-all-start.2 = ((bf16[16,32,384]{2,1,0:T(8,128)(2,1)}), bf16[16,32,384]{2,1,0:T(8,128)(2,1)S(1)}, u32[]{:S(2)}, u32[]{:S(2)}) async-start(bf16[16,32,384]{2,1,0:T(8,128)(2,1)} %gather_fusion.1), calls=%async_computation.2 | async-start | bytes 786432 | tf_op jit(solution)/shard_map/all_to_all | solution.py:93
  70.6 47.2 %reduce-scatter.2.cloned.1.call-start = ((), (), s32[]{:S(2)}) async-start(), calls=%async_computation.4 | async-start | bytes 2621440 | tf_op jit(solution)/shard_map/reduce_scatter | solution.py:108
  71.0 4.5 %copy-start.3 = (f32[3,512,512]{1,2,0:T(8,128)S(1)}, f32[3,512,512]{1,2,0:T(8,128)}, u32[]{:S(2)}) copy-start(f32[3,512,512]{1,2,0:T(8,128)} %copy-done.2) | copy-start | bytes 9437188
  71.0 4.5 %copy-start.6 = (bf16[512,384]{0,1:T(8,128)(2,1)S(1)}, bf16[512,384]{0,1:T(8,128)(2,1)}, u32[]{:S(2)}) copy-start(bf16[512,384]{0,1:T(8,128)(2,1)} %copy.56) | copy-start | bytes 1179652
  72.9 1.7 %copy-start.4 = (f32[3,512,512]{1,2,0:T(8,128)}, f32[3,512,512]{1,2,0:T(8,128)S(1)}, u32[]{:S(2)}) copy-start(f32[3,512,512]{1,2,0:T(8,128)S(1)} %get-tuple-element.19) | copy-start | bytes 9437188
Sparse Core Ops, SparseCore 0:
  8.9 25.2 all-gather.2
  88.5 29.2 reduce-scatter.1
